TPU v7x, 32 devices: a whole 2x2x4 slice. The times are simulated.
32 devices in a mesh: rep: 2 (over x), fs: 8 (over z, y), tp: 2 (over core).
Axes of the slice: x: 2, y: 2, z: 4, core: 2. Of those that a mesh axis runs over, the one named last changes fastest.
Arguments:
- tokens: bfloat16 [4096, 2048], P(('rep', 'fs')), may hold values from -6 to 6
- mid_tokens: bfloat16 [4096, 2048], P(('rep', 'fs')), may hold values from -6 to 6
- out_grad: bfloat16 [4096, 2048], P(('rep', 'fs')), may hold values from -6 to 6
- gate_first: bfloat16 [2048, 3072], P('fs', 'tp'), may hold values from -0.125 to 0.125
- up_first: bfloat16 [2048, 3072], P('fs', 'tp'), may hold values from -0.125 to 0.125
- down_first: bfloat16 [3072, 2048], P('tp', 'fs'), may hold values from -0.109375 to 0.109375
- gate_second: bfloat16 [2048, 3072], P('fs', 'tp'), may hold values from -0.125 to 0.125
- up_second: bfloat16 [2048, 3072], P('fs', 'tp'), may hold values from -0.125 to 0.125
- down_second: bfloat16 [3072, 2048], P('tp', 'fs'), may hold values from -0.109375 to 0.109375
Outputs:
- input_grad: bfloat16 [4096, 2048], P(('rep', 'fs'))
- down_grad: float32 [3072, 2048], P('tp', 'fs')
- row_norms: float32 [3072], P('tp')
All inputs are finite; a program needn't handle non-finite values.
Results may differ from a plain program's by a relative error of at most 0.025.
Values may be sent and summed in bfloat16 or wider, within the bound.
A program may use at most 128 MiB of HBM per device.

v0:
```python
import functools

import jax
import jax.numpy as jnp
from jax import lax
from jax.experimental import pallas as pl
from jax.experimental.pallas import tpu as pltpu
from jax.sharding import PartitionSpec as P

eps = 1e-06
f32, bf16 = jnp.float32, jnp.bfloat16


def kernel(sizes, tok, mid, cot, g1, u1, v1, g2, u2, v2, out, grad, norms, full1, downs1, full2, downs2, toks, mids, cots, mgs, xb, hidden, d_gate, d_up, mgt, gates, uppers, part, got1, snd2, got2, dn, rs_out, rs_in, gb, nb, w_send, w_recv, own_sem, x_send, x_recv, s1_send, s1_recv, s2_send, s2_recv, s3_send, s3_recv, r_send, r_recv, g_send, g_recv, n_send, n_recv):
    R, F, T, n, D, H, pieces = sizes
    S, half, C, width = D // F, D // F // 2, D // T, H // pieces
    both = 2 if pieces > 1 else 1
    r, f, t = (lax.axis_index(a) for a in ("rep", "fs", "tp"))

    def fs_at(position):
        q = lax.rem(position + 2 * F, F)
        hi = q // (F // 2)
        return (1 - hi) * 2 * q + hi * (2 * (F - 1 - q) + 1)

    odd = lax.rem(f, 2)
    p = (1 - odd) * (f // 2) + odd * (F - 1 - f // 2)
    side = (fs_at(p + 1), fs_at(p - 1))

    barrier = pltpu.get_barrier_semaphore()
    for axis, size, me in (("rep", R, r), ("fs", F, f), ("tp", T, t)):
        for k in range(1, size):
            pl.semaphore_signal(barrier, inc=1, device_id={axis: lax.rem(me + k, size)}, device_id_type=pl.DeviceIdType.MESH)
    pl.semaphore_wait(barrier, R + F + T - 3)

    def remote(src, dst, send, recv, **where):
        return pltpu.make_async_remote_copy(src_ref=src, dst_ref=dst, send_sem=send, recv_sem=recv, device_id=where, device_id_type=pl.DeviceIdType.MESH)

    fulls = ((full1, downs1), (full2, downs2))

    second_gu, second_d = (1, 0, both, 2 * H // both, 0), (1, 1, pieces, width, both)
    first_gu, first_d = (0,) + second_gu[1:], (0,) + second_d[1:]

    def ring(phase, d, distance, step, piece):
        b, which, count, wide, sem = phase
        owner = fs_at(p - distance if d == 0 else p + distance)
        rows = pl.ds(pl.multiple_of(owner * S + d * half, half), half)
        ref = fulls[b][which].at[rows]
        if count > 1:
            ref = fulls[b][which].at[rows, pl.ds(pl.multiple_of(piece * wide, 128), wide)]
        return remote(ref, ref, w_send.at[b, which, d], w_recv.at[b, d, step, sem + piece], fs=side[d])

    def start_ring(phase):
        for piece in range(phase[2]):
            for d in (0, 1):
                ring(phase, d, 0, 0, piece).start()

    def serve(phase, lo, hi, of):
        relays = (F - 2) * phase[2]

        @pl.loop(relays * lo // of, relays * hi // of)
        def _(k):
            step, piece = k // phase[2], lax.rem(k, phase[2])
            for d in (0, 1):
                ring(phase, d, step + 1, step, piece).wait_recv()
                ring(phase, d, step + 1, step + 1, piece).start()

    def end_ring(phase):
        for piece in range(phase[2]):
            for d in (0, 1):
                ring(phase, d, F - 1, F - 2, piece).wait_recv()

    def drain(b):
        for which in (0, 1):
            whole = fulls[b][which].at[pl.ds(0, (F - 1) * half)]
            for d in (0, 1):
                remote(whole, whole, w_send.at[b, which, d], w_recv.at[b, d, 0, 0], fs=side[d]).wait_send()

    mine = pl.ds(pl.multiple_of(r * n, n), n)
    pairs = (mids, cots, toks, mgs)
    held = pl.ds(pl.multiple_of(f * S, S), S)
    def pair_loads(g, u, full):
        if H % 128 > 0:
            return [(g, full.at[held])]
        taken = pl.ds(pl.multiple_of(r * H, 128), H)
        return [(g.at[:, taken], full.at[held, pl.ds(0, H)]), (u.at[:, taken], full.at[held, pl.ds(H, H)])]

    wanted = pair_loads(g2, u2, full2)
    ahead = len(wanted)
    wanted += [(mid, mids.at[mine]), (cot, cots.at[mine]), (tok, toks.at[mine]), (v2, downs2.at[held]), (v1, downs1.at[held])]
    wanted += pair_loads(g1, u1, full1)
    loads = [pltpu.make_async_copy(src, dst, own_sem.at[i]) for i, (src, dst) in enumerate(wanted)]
    for c in loads:
        c.start()

    def swap(i):
        return [remote(pairs[i].at[mine], pairs[i].at[mine], x_send.at[i, k - 1], x_recv.at[i, k - 1], rep=lax.rem(r + k, R)) for k in range(1, R)]

    def swap_in(i):
        for k in range(1, R):
            rows = pl.ds(pl.multiple_of(lax.rem(r + R - k, R) * n, n), n)
            remote(pairs[i].at[rows], pairs[i].at[rows], x_send.at[i, k - 1], x_recv.at[i, k - 1], rep=lax.rem(r + k, R)).wait_recv()

    for c in loads[:ahead]:
        c.wait()
    start_ring(second_gu)
    for i in range(3):
        loads[ahead + i].wait()
        for c in swap(i):
            c.start()
    for c in loads[ahead + 3 :]:
        c.wait()

    def normalise(pair):
        @pl.loop(0, R * n // 32)
        def _(i):
            rows = pl.ds(pl.multiple_of(i * 32, 32), 32)
            u = pair[rows, :].astype(f32)
            xb[rows, :] = (u * lax.rsqrt(jnp.mean(u * u, axis=1, keepdims=True) + eps)).astype(bf16)

    chunk = 256 if H % 256 == 0 else 128 if H % 128 == 0 else H

    def cols(which, j):
        if chunk == H:
            return pl.ds(which * H, H)
        return pl.ds(pl.multiple_of(which * H + j * chunk, 128), chunk)

    def forward(full):
        @pl.loop(0, H // chunk)
        def _(j):
            gate = jnp.dot(xb[...], full[:, cols(0, j)], preferred_element_type=f32)
            upper = jnp.dot(xb[...], full[:, cols(1, j)], preferred_element_type=f32)
            hidden[:, cols(0, j)] = (gate * jax.nn.sigmoid(gate) * upper).astype(bf16)
            gates[:, cols(0, j)] = gate
            uppers[:, cols(0, j)] = upper

    def backed(downs, c_ref):
        @pl.loop(0, H // chunk)
        def _(j):
            gate, upper = gates[:, cols(0, j)], uppers[:, cols(0, j)]
            back = 0.5 * jnp.dot(c_ref[...], downs[:, cols(0, j)], preferred_element_type=f32)
            logistic = jax.nn.sigmoid(gate)
            d_gate[:, cols(0, j)] = (back * upper * logistic * (1.0 + gate * (1.0 - logistic))).astype(bf16)
            d_up[:, cols(0, j)] = (back * gate * logistic).astype(bf16)

    dims = (((1,), (1,)), ((), ()))

    def backward(full, lo, hi):
        @pl.loop(lo, hi)
        def _(j):
            rows = pl.ds(pl.multiple_of(j * 256, 256), 256)
            total = lax.dot_general(d_gate[...], full[rows, 0:H], dims, preferred_element_type=f32)
            total = total + lax.dot_general(d_up[...], full[rows, H : 2 * H], dims, preferred_element_type=f32)
            part[:, rows] = total.astype(bf16)

    def block_of(k):
        return pl.ds(pl.multiple_of(k * C, 128), C)

    def stage1(b):
        return [remote(part.at[:, block_of(lax.rem(t + k, T))], got1.at[b, k - 1], s1_send.at[b, k - 1], s1_recv.at[b, k - 1], tp=lax.rem(t + k, T)) for k in range(1, T)]

    def stage2(b):
        return [remote(snd2.at[k - 1], got2.at[b, k - 1], s2_send.at[b, k - 1], s2_recv.at[b, k - 1], rep=lax.rem(r + k, R)) for k in range(1, R)]

    def stage3(b, owner):
        ref = dn.at[b, :, block_of(owner)]
        return lambda k: remote(ref, ref, s3_send.at[b, k - 1], s3_recv.at[b, k - 1], tp=lax.rem(t + k, T))

    def summed(b, base, i):
        rows = pl.ds(pl.multiple_of(base * n + i * 32, 32), 32)
        total = part[rows, block_of(t)].astype(f32)
        for k in range(T - 1):
            total = total + got1[b, k, rows, :].astype(f32)
        return total

    def reduce_tp(b):
        for c in stage1(b):
            c.wait()
        for k in range(1, R):
            @pl.loop(0, n // 32)
            def _(i, k=k):
                snd2[k - 1, pl.ds(pl.multiple_of(i * 32, 32), 32), :] = summed(b, lax.rem(r + k, R), i).astype(bf16)
        for c in stage2(b):
            c.start()

    def reduce_rep(b):
        for c in stage2(b):
            c.wait()

        @pl.loop(0, n // 32)
        def _(i):
            rows = pl.ds(pl.multiple_of(i * 32, 32), 32)
            total = summed(b, r, i)
            for k in range(R - 1):
                total = total + got2[b, k, rows, :].astype(f32)
            dn[b, rows, block_of(t)] = total.astype(bf16)

        for k in range(1, T):
            stage3(b, t)(k).start()

    def finish(b, pair, carried, result, offset):
        for k in range(1, T):
            stage3(b, lax.rem(t + T - k, T))(k).wait_recv()
            stage3(b, t)(k).wait_send()

        @pl.loop(0, n // 32)
        def _(i):
            rows = pl.ds(pl.multiple_of(i * 32, 32), 32)
            wide = pl.ds(pl.multiple_of(r * n + i * 32, 32), 32)
            u = pair[wide, :].astype(f32)
            scale = lax.rsqrt(jnp.mean(u * u, axis=1, keepdims=True) + eps)
            normed = u * scale
            d = dn[b, rows, :].astype(f32)
            d_u = carried[wide, :].astype(f32) + scale * (d - normed * jnp.mean(d * normed, axis=1, keepdims=True))
            result[pl.ds(pl.multiple_of(offset + i * 32, 32), 32), :] = d_u.astype(bf16)

    serve(second_gu, 0, 10, 12)
    swap_in(0)
    normalise(mids)
    serve(second_gu, 10, 12, 12)
    start_ring(second_d)
    end_ring(second_gu)
    serve(second_d, 0, 3, 18)
    forward(full2)
    serve(second_d, 3, 18, 18)
    start_ring(first_gu)
    swap_in(1)
    end_ring(second_d)
    backed(downs2, cots)
    serve(first_gu, 0, 1, 12)
    backward(full2, 0, D // 512)
    serve(first_gu, 1, 2, 12)
    backward(full2, D // 512, D // 256)
    for c in stage1(1):
        c.start()
    serve(first_gu, 2, 3, 12)
    reduce_tp(1)
    serve(first_gu, 3, 4, 12)
    swap_in(2)
    normalise(toks)
    serve(first_gu, 4, 6, 12)
    reduce_rep(1)
    serve(first_gu, 6, 7, 12)
    finish(1, mids, cots, mgs, r * n)
    for c in swap(3):
        c.start()
    serve(first_gu, 7, 12, 12)
    start_ring(first_d)
    end_ring(first_gu)

    forward(full1)
    serve(first_d, 0, 6, 18)
    swap_in(3)

    @pl.loop(0, D // 256)
    def _(j):
        part_cols = pl.ds(pl.multiple_of(j * 256, 256), 256)
        mgt[part_cols, :] = mgs[:, part_cols].T

    serve(first_d, 6, 18, 18)

    def strip(piece):
        return pl.ds(pl.multiple_of(piece * width, 128), width) if pieces > 1 else slice(None)

    def product(d, position, piece):
        rows = pl.ds(pl.multiple_of(fs_at(position) * S + d * half, half), half)
        return 0.5 * jnp.dot(mgt[rows, :], hidden[:, strip(piece)], preferred_element_type=f32)

    def view(ref, piece):
        return ref.at[:, strip(piece)] if pieces > 1 else ref

    def rs(d, s, piece):
        return remote(view(rs_out.at[d, s], piece), view(rs_in.at[d, s], piece), r_send.at[d, s, piece], r_recv.at[d, s, piece], fs=side[d])

    def passed(lo, hi):
        @pl.loop(1 + (F - 2) * lo // 6, 1 + (F - 2) * hi // 6)
        def _(s):
            for piece in range(pieces):
                for d in (0, 1):
                    value = product(d, p - 1 - s if d == 0 else p + 1 + s, piece)
                    rs(d, s - 1, piece).wait_recv()
                    rs_out[d, s, :, strip(piece)] = (value + rs_in[d, s - 1, :, strip(piece)].astype(f32)).astype(bf16)
                    rs(d, s, piece).start()

    for piece in range(pieces):
        for d in (0, 1):
            rs_out[d, 0, :, strip(piece)] = product(d, p - 1 if d == 0 else p + 1, piece).astype(bf16)
            rs(d, 0, piece).start()
    end_ring(first_d)
    backed(downs1, mgs)
    passed(0, 1)
    backward(full1, 0, D // 512)
    passed(1, 2)
    backward(full1, D // 512, D // 256)
    for c in stage1(0):
        c.start()
    passed(2, 3)
    reduce_tp(0)
    passed(3, 6)

    def trade(owner, piece):
        ref = view(gb.at[owner], piece)
        return lambda k: remote(ref, ref, g_send.at[k - 1, piece], g_recv.at[k - 1, piece], rep=lax.rem(r + k, R))

    for piece in range(pieces):
        for d in (0, 1):
            value = product(d, p, piece)
            rs(d, F - 2, piece).wait_recv()
            gb[r, pl.ds(d * half, half), strip(piece)] = (value + rs_in[d, F - 2, :, strip(piece)].astype(f32)).astype(bf16)
        for k in range(1, R):
            trade(r, piece)(k).start()
    reduce_rep(0)
    finish(0, toks, mgs, out, 0)
    for piece in range(pieces):
        for k in range(1, R):
            trade(lax.rem(r + R - k, R), piece)(k).wait_recv()
            trade(r, piece)(k).wait_send()
    for k in range(R):
        g = gb[k].astype(f32)
        grad[:, k * H : (k + 1) * H] = g
        nb[f, :, k * H : (k + 1) * H] = jnp.sum(g * g, axis=0, keepdims=True)

    def tell(owner):
        return lambda k: remote(nb.at[owner], nb.at[owner], n_send.at[k - 1], n_recv.at[k - 1], fs=lax.rem(f + k, F))

    for k in range(1, F):
        tell(f)(k).start()
    for b in (0, 1):
        drain(b)
    for i in range(4):
        for c in swap(i):
            c.wait_send()

    @pl.loop(0, F - 1)
    def _(s):
        for piece in range(pieces):
            for d in (0, 1):
                rs(d, s, piece).wait_send()

    for k in range(1, F):
        tell(lax.rem(f + F - k, F))(k).wait_recv()
        tell(f)(k).wait_send()
    total = nb[0]
    for k in range(1, F):
        total = total + nb[k]
    norms[...] = total


def on_device(sizes, tokens, mid_tokens, out_grad, gate_first, up_first, down_first, gate_second, up_second, down_second):
    R, F, T, n, D, H, pieces = sizes
    S, half = D // F, D // F // 2
    start = lax.axis_index("rep") * H

    def own(gate_w, up_w, down_w):
        down = lax.dynamic_slice_in_dim(down_w, start, H, 0).T
        if H % 128 == 0:
            return gate_w, up_w, down
        pair = [lax.dynamic_slice_in_dim(w, start, H, 1) for w in (gate_w, up_w)]
        return jnp.concatenate(pair, axis=1), up_w, down

    dma = pltpu.SemaphoreType.DMA
    m = R * n
    any_space = pl.BlockSpec(memory_space=pl.ANY)
    vmem = pl.BlockSpec(memory_space=pltpu.VMEM)
    d_input, grad, norms = pl.pallas_call(
        functools.partial(kernel, sizes),
        out_shape=(
            jax.ShapeDtypeStruct((n, D), bf16),
            jax.ShapeDtypeStruct((S, R * H), f32),
            jax.ShapeDtypeStruct((1, R * H), f32),
        ),
        in_specs=[any_space] * 9,
        out_specs=(vmem, vmem, vmem),
        scratch_shapes=[
            pltpu.VMEM((D, 2 * H), bf16),
            pltpu.VMEM((D, H), bf16),
            pltpu.VMEM((D, 2 * H), bf16),
            pltpu.VMEM((D, H), bf16),
            pltpu.VMEM((m, D), bf16),
            pltpu.VMEM((m, D), bf16),
            pltpu.VMEM((m, D), bf16),
            pltpu.VMEM((m, D), bf16),
            pltpu.VMEM((m, D), bf16),
            pltpu.VMEM((m, H), bf16),
            pltpu.VMEM((m, H), bf16),
            pltpu.VMEM((m, H), bf16),
            pltpu.VMEM((D, m), bf16),
            pltpu.VMEM((m, H), f32),
            pltpu.VMEM((m, H), f32),
            pltpu.VMEM((m, D), bf16),
            pltpu.VMEM((2, T - 1, m, D // T), bf16),
            pltpu.VMEM((R - 1, n, D // T), bf16),
            pltpu.VMEM((2, R - 1, n, D // T), bf16),
            pltpu.VMEM((2, n, D), bf16),
            pltpu.VMEM((2, F - 1, half, H), bf16),
            pltpu.VMEM((2, F - 1, half, H), bf16),
            pltpu.VMEM((R, S, H), bf16),
            pltpu.VMEM((F, 1, R * H), f32),
            dma((2, 2, 2)),
            dma((2, 2, F - 1, pieces + (2 if pieces > 1 else 1))),
            dma((9,)),
            dma((4, R - 1)),
            dma((4, R - 1)),
            dma((2, T - 1)),
            dma((2, T - 1)),
            dma((2, R - 1)),
            dma((2, R - 1)),
            dma((2, T - 1)),
            dma((2, T - 1)),
            dma((2, F - 1, pieces)),
            dma((2, F - 1, pieces)),
            dma((R - 1, pieces)),
            dma((R - 1, pieces)),
            dma((F - 1,)),
            dma((F - 1,)),
        ],
        compiler_params=pltpu.CompilerParams(
            collective_id=0, has_side_effects=True, vmem_limit_bytes=67043328
        ),
    )(
        tokens,
        mid_tokens,
        out_grad,
        *own(gate_first, up_first, down_first),
        *own(gate_second, up_second, down_second),
    )
    return d_input, grad.T, norms.reshape(-1)


def solution(mesh):
    R, F, T = (mesh.shape[a] for a in ("rep", "fs", "tp"))

    def whole(tokens, mid_tokens, out_grad, gate_first, *rest):
        D, FF = gate_first.shape
        sizes = (R, F, T, tokens.shape[0] // (R * F), D, FF // (T * R), 3 if F <= 8 and FF // (T * R) % 384 == 0 else 1)
        return jax.shard_map(
            functools.partial(on_device, sizes),
            mesh=mesh,
            in_specs=(P(("rep", "fs"), None),) * 3 + (P("fs", "tp"), P("fs", "tp"), P("tp", "fs")) * 2,
            out_specs=(P(("rep", "fs"), None), P("tp", "fs"), P("tp")),
            check_vma=False,
        )(tokens, mid_tokens, out_grad, gate_first, *rest)

    return whole
```

profile of v0, /device:TPU:0, one launch (start us, length us, event | category | flops | bytes accessed | tf_op | source)
XLA Modules:
  0.0 244.3 jit_solution(9462708712932138181)
XLA Ops:
  0.6 1.2 constant_dynamic-slice_fusion
  1.8 0.9 copy.16
  2.7 0.9 copy.15
  3.6 235.9 %shard_map.112 = (bf16[256,2048]{1,0:T(8,128)(2,1)}, f32[256,1536]{1,0:T(8,128)}, f32[1,1536]{1,0:T(1,128)}) custom-call(bf16[256,2048]{1,0:T(8,128)(2,1)} %tok.1, bf16[256,2048]{1,0:T(8,128)(2,1)} %mid.1, bf16[256,2048]{1,0:T(8,128)(2,1)} %cot.1, bf16[256,1536]{1,0:T(8,128)(2,1)} %g1.1, bf16[256,1536]{1,0:T(8,128)(2,1)} %u1_.1, bf16[256,768]{1,0:T(8,128)(2,1)} %bitcast.5, ...), custom_call_target="tpu_custom_call" | custom-call | tf_op jit(solution)/shard_map/pallas_call | solution.py:364
  239.6 0.0 copy-start.1
  239.6 0.0 copy-start
  239.6 3.1 %copy.14 = f32[1536,256]{1,0:T(8,128)} copy(f32[1536,256]{0,1:T(8,128)} %bitcast.3) | data formatting | bytes 3145728
  242.7 0.0 copy-done.1
  242.7 0.6 reduce
  243.4 0.0 copy-done
  243.4 1.0 copy.18
Async XLA Ops:
  239.6 3.1 %copy-start.1 = (f32[1,1536]{1,0:T(1,128)S(1)}, f32[1,1536]{1,0:T(1,128)}, u32[]{:S(2)}) copy-start(f32[1,1536]{1,0:T(1,128)} %get-tuple-element.8) | copy-start | bytes 18436
  239.6 3.7 %copy-start = (bf16[256,2048]{1,0:T(8,128)(2,1)S(1)}, bf16[256,2048]{1,0:T(8,128)(2,1)}, u32[]{:S(2)}) copy-start(bf16[256,2048]{1,0:T(8,128)(2,1)} %get-tuple-element.17) | copy-start | bytes 3145732
where the time goes:
time: 244 us
  Pallas kernels  236 us (97%)
  local copies, waits for them, and re-layouts  7.1 us (3%)
    pallas_call x1, Pallas kernels, on_device(): pl.pallas_call(functools.partial(kernel, sizes), out_shape=(jax.ShapeDtyp...  236 us
    unnamed x8, local copies, waits for them, and re-layouts  5.93 us

commit v1 on v0

--- a/solution.py
+++ b/solution.py
@@ -426,14 +426,598 @@
     return d_input, grad.T, norms.reshape(-1)
 
 
+def square_kernel(sizes, tok, mid, cot, g1, u1, v1, g2, u2, v2, out, grad, norms, gu, dd, acts, xb, acc, bk, dg, hT, part, sib, xs, xr, zs, zr, dbuf, scb, ps, pr, obs, obr, gys, gyr, g2s, g2r, gzs, gq, nb, own_sem, wz_send, wz_recv, wy_send, wy_recv, a_send, a_recv, s_send, s_recv, x_send, x_recv, z_send, z_recv, p_send, p_recv, o_send, o_recv, gy_send, gy_recv, g2_send, g2_recv, gz_send, gz_recv, gx_send, gx_recv, n_send, n_recv):
+    R, F, T, n, D, H = sizes
+    S, half, h = D // F, D // 2, n // 2
+    r, f, t = (lax.axis_index(a) for a in ("rep", "fs", "tp"))
+    z, y = f // 2, lax.rem(f, 2)
+    zl, zh = lax.rem(z, 2), z // 2
+
+    def fs_of(k, side):
+        return 2 * (2 * lax.rem(zh + k // 2, 2) + lax.rem(zl + k % 2, 2)) + side
+
+    to_x, to_y, to_s = {"rep": 1 - r}, {"fs": fs_of(0, 1 - y)}, {"tp": 1 - t}
+    to_z = [None] + [{"fs": fs_of(k, y)} for k in (1, 2, 3)]
+    inn = lax.rem(zl + zh, 2)
+    inner, outer = inn == 1, inn == 0
+    me, jx, jz, jd = 2 * r + zl, 2 * (1 - r) + zl, 2 * r + 1 - zl, 2 * (1 - r) + 1 - zl
+
+    barrier = pltpu.get_barrier_semaphore()
+    for axis, size, at in (("rep", R, r), ("fs", F, f), ("tp", T, t)):
+        for k in range(1, size):
+            pl.semaphore_signal(barrier, inc=1, device_id={axis: lax.rem(at + k, size)}, device_id_type=pl.DeviceIdType.MESH)
+
+    def at(start, size, step=8):
+        return pl.ds(pl.multiple_of(start, step), size)
+
+    def remote(src, dst, send, recv, where):
+        return pltpu.make_async_remote_copy(src_ref=src, dst_ref=dst, send_sem=send, recv_sem=recv, device_id=where, device_id_type=pl.DeviceIdType.MESH)
+
+    weights = ((g1, u1, v1), (g2, u2, v2))
+    fields = (mid, cot, tok)
+
+    def source(b, p, q):
+        ref = weights[b][p]
+        return ref.at[at(q * H, H)] if p == 2 else ref.at[:, at(q * H, H, 128)]
+
+    def place(b, p, owner):
+        if p == 2:
+            return dd.at[b, :, at(owner * S, S, 128)]
+        return gu.at[b, at(owner * S, S), pl.ds(p * H, H)]
+
+    loads = {}
+    for i in range(3):
+        loads["a", i] = pltpu.make_async_copy(fields[i], acts.at[i, at(me * n, n)], own_sem.at[i])
+    for b in (1, 0):
+        for p in range(3):
+            loads["w", b, p] = pltpu.make_async_copy(source(b, p, me), place(b, p, f), own_sem.at[3 + 3 * b + p])
+    for c in loads.values():
+        c.start()
+    pl.semaphore_wait(barrier, R + F + T - 3)
+
+    def w_first(b, p, k):
+        q = me if k == 2 else jz
+        return remote(source(b, p, q), place(b, p, f), wz_send.at[b, p, k], wz_recv.at[b, p, k], to_z[k])
+
+    def w_relay(b, p):
+        ref = place(b, p, fs_of(1, y))
+        return remote(ref, ref, wz_send.at[b, p, 0], wz_recv.at[b, p, 3], to_z[2])
+
+    def w_cross(b, p, k):
+        ref = place(b, p, fs_of(k, y))
+        return remote(source(b, p, me) if isinstance(k, int) and k == 0 else ref, ref, wy_send.at[b, p, k], wy_recv.at[b, p, k], to_y)
+
+    def w_arrived(b, p, k):
+        ref = place(b, p, fs_of(k, y))
+        remote(ref, ref, wz_send.at[b, p, k], wz_recv.at[b, p, k], to_z[1]).wait_recv()
+
+    def crossed(b, pieces, k):
+        for p in pieces:
+            ref = place(b, p, fs_of(k, 1 - y))
+            remote(ref, ref, wy_send.at[b, p, k], wy_recv.at[b, p, k], to_y).wait_recv()
+
+    def serve(b, pieces, k, near=False):
+        for p in pieces:
+            w_arrived(b, p, k)
+            if near:
+                @pl.when(inner)
+                def _(p=p):
+                    w_relay(b, p).start()
+            w_cross(b, p, k).start()
+
+    mine, other = at(t * half, half, 128), at((1 - t) * half, half, 128)
+
+    def rows_of(j):
+        return at(j * n, n)
+
+    def a_copy(i, kind):
+        if kind < 2:
+            dst = acts.at[i, rows_of(me), mine]
+            return remote(fields[i].at[:, mine] if i < 3 else dst, dst, a_send.at[i, kind], a_recv.at[i, kind], (to_z[1], to_x)[kind])
+        ref = acts.at[i, rows_of({2: jz, 3: jz, 4: jx, 5: jd, 6: me}[kind]), mine]
+        return remote(ref, ref, a_send.at[i, kind], a_recv.at[i, kind], to_x if kind == 2 else to_s)
+
+    def a_arrived(i, kind):
+        j = (jz, jx, jd, jz, jx, jd, me)[kind]
+        ref = acts.at[i, rows_of(j), mine if kind < 3 else other]
+        remote(ref, ref, a_send.at[i, kind], a_recv.at[i, kind], to_x).wait_recv()
+
+    def a_zn(i):
+        a_arrived(i, 0)
+        a_copy(i, 2).start()
+        a_copy(i, 3).start()
+
+    def a_x(i):
+        a_arrived(i, 1)
+        a_copy(i, 4).start()
+
+    def a_d(i):
+        a_arrived(i, 2)
+        a_copy(i, 5).start()
+
+    def a_s(i):
+        for kind in (3, 4, 5) + ((6,) if i == 3 else ()):
+            a_arrived(i, kind)
+
+    def normalise(i, lo, hi):
+        @pl.loop(lo * n // 32, hi * n // 32)
+        def _(c):
+            rows = at(c * 32, 32)
+            u = acts[i, rows, :].astype(f32)
+            xb[rows, :] = (u * lax.rsqrt(jnp.mean(u * u, axis=1, keepdims=True) + eps)).astype(bf16)
+
+    nt = (((1,), (1,)), ((), ()))
+
+    def forward(b, owner, first=False):
+        cut = at(owner * S, S, 128)
+
+        @pl.loop(0, 2 * H // 256)
+        def _(j):
+            cols = at(j * 256, 256, 128)
+            value = jnp.dot(xb[:, cut], gu[b, at(owner * S, S), cols], preferred_element_type=f32)
+            acc[:, cols] = value if first else acc[:, cols] + value
+
+    def backed(b, i, owner, first=False):
+        cut = at(owner * S, S, 128)
+
+        @pl.loop(0, 2)
+        def _(j):
+            rows = at(j * 2 * n, 2 * n)
+            value = lax.dot_general(acts[i, rows, cut], dd[b, :, cut], nt, preferred_element_type=f32)
+            bk[rows, :] = value if first else bk[rows, :] + value
+
+    def hidden():
+        @pl.loop(0, 4 * n // 128)
+        def _(c):
+            rows = at(c * 128, 128)
+            gate = acc[rows, 0:H]
+            hT[:, at(c * 128, 128, 128)] = (gate * jax.nn.sigmoid(gate) * acc[rows, H : 2 * H]).astype(bf16).T
+
+    def elementwise():
+        @pl.loop(0, 4 * n // 64)
+        def _(c):
+            rows = at(c * 64, 64)
+            gate, upper, back = acc[rows, 0:H], acc[rows, H : 2 * H], 0.5 * bk[rows, :]
+            logistic = jax.nn.sigmoid(gate)
+            dg[rows, 0:H] = (back * upper * logistic * (1.0 + gate * (1.0 - logistic))).astype(bf16)
+            dg[rows, H : 2 * H] = (back * gate * logistic).astype(bf16)
+
+    def partial(b, side, c):
+        rows = at(side * 2 * n, 2 * n)
+
+        @pl.loop(0, half // 256)
+        def _(j):
+            wide = c * half + j * 256
+            total = lax.dot_general(dg[rows, :], gu[b, at(wide, 256), :], nt, preferred_element_type=f32)
+            part[rows, at(wide, 256, 128)] = total.astype(bf16)
+
+    def sibling(b, i, side):
+        rows = at(side * 2 * n, 2 * n)
+        return remote(part.at[rows, other], sib.at[b, rows], s_send.at[b, i], s_recv.at[b, i], to_s)
+
+    def partials(b, between=None):
+        for i, side in enumerate((1 - r, r)):
+            partial(b, side, 1 - t)
+            sibling(b, i, side).start()
+            partial(b, side, t)
+            if between is not None:
+                between(i)
+
+    def x_copy(b, piece):
+        rows = pl.ds(piece * h, h)
+        return remote(xs.at[rows], xr.at[b, rows], x_send.at[b, piece], x_recv.at[b, piece], to_x)
+
+    def z_copy(b, piece):
+        rows = pl.ds(piece * h, h)
+        return remote(zs.at[rows], zr.at[b, rows], z_send.at[b, piece], z_recv.at[b, piece], to_z[1])
+
+    def own_sum(b, rows):
+        return part[rows, mine].astype(f32) + sib[b, rows, :].astype(f32)
+
+    def x_step(b):
+        sibling(b, 0, 1 - r).wait_recv()
+        for piece in range(4):
+            base = (jd if piece < 2 else jx) * n + (piece % 2) * h
+
+            @pl.loop(0, h // 32)
+            def _(c, base=base, piece=piece):
+                xs[at(piece * h + c * 32, 32), :] = own_sum(b, at(base + c * 32, 32)).astype(bf16)
+
+            x_copy(b, piece).start()
+        sibling(b, 1, r).wait_recv()
+
+    def z_step(b, piece):
+        x_copy(b, piece).wait_recv()
+
+        @pl.loop(0, h // 32)
+        def _(c):
+            rows = at(piece * h + c * 32, 32)
+            total = own_sum(b, at(jz * n + piece * h + c * 32, 32)) + xr[b, rows, :].astype(f32)
+            zs[rows, :] = total.astype(bf16)
+
+        z_copy(b, piece).start()
+
+    def sum_send(b, buf, piece, base, extra, copy):
+        @pl.loop(0, h // 32)
+        def _(c):
+            total = own_sum(b, at(base + c * 32, 32))
+            if extra is not None:
+                total = total + extra[b, at(c * 32, 32), :].astype(f32)
+            buf[at(piece * h + c * 32, 32), :] = total.astype(bf16)
+
+        copy(b, piece).start()
+
+    def spread(i):
+        sibling(0, i, (1 - r, r)[i]).wait_recv()
+        if i == 0:
+            sum_send(0, xs, 0, jd * n, None, x_copy)
+            sum_send(0, zs, 0, jd * n + h, None, z_copy)
+            sum_send(0, xs, 1, jx * n, None, x_copy)
+        else:
+            sum_send(0, zs, 1, jz * n + h, None, z_copy)
+
+    def spread_end():
+        x_copy(0, 0).wait_recv()
+        sum_send(0, zs, 2, jz * n, xr, z_copy)
+        z_copy(0, 0).wait_recv()
+        sum_send(0, xs, 2, jx * n + h, zr, x_copy)
+
+    def finish(b, ui, ci, parts, store):
+        for piece, (px, pz) in enumerate(parts):
+            x_copy(b, px).wait_recv()
+            z_copy(b, pz).wait_recv()
+
+            @pl.loop(piece * h // 32, (piece + 1) * h // 32)
+            def _(c, piece=piece, px=px, pz=pz):
+                rows, wide = at(c * 32, 32), at(me * n + c * 32, 32)
+                from_x, from_z = (at((q - piece) * h + c * 32, 32) for q in (px, pz))
+                d = own_sum(b, wide) + xr[b, from_x, :].astype(f32) + zr[b, from_z, :].astype(f32)
+                u = acts[ui, wide, :].astype(f32)
+                scale = lax.rsqrt(jnp.mean(u * u, axis=1, keepdims=True) + eps)
+                normed = acts[ui, wide, mine].astype(f32) * scale
+                dbuf[rows, :] = d
+                ps[rows, :] = jnp.broadcast_to(jnp.sum(d * normed, axis=1, keepdims=True), (32, 128))
+                scb[rows, :] = jnp.broadcast_to(scale, (32, 128))
+
+        tell = remote(ps, pr.at[b], p_send.at[b], p_recv.at[b], to_s)
+        tell.start()
+        tell.wait()
+
+        @pl.loop(0, n // 32)
+        def _(c):
+            rows, wide = at(c * 32, 32), at(me * n + c * 32, 32)
+            scale = scb[rows, 0:1]
+            normed = acts[ui, wide, mine].astype(f32) * scale
+            mean = (ps[rows, 0:1] + pr[b, rows, 0:1]) * (1.0 / D)
+            d_u = acts[ci, wide, mine].astype(f32) + scale * (dbuf[rows, :] - normed * mean)
+            store(rows, wide, d_u.astype(bf16))
+
+    def product(k, side):
+        cut = at(fs_of(k, side) * S, S, 128)
+        return 0.5 * jnp.dot(hT[...], acts[3, :, cut], preferred_element_type=f32)
+
+    def gy(k):
+        return remote(gys.at[k], gyr.at[k], gy_send.at[k], gy_recv.at[k], to_y)
+
+    def gfar(i):
+        return remote(g2s.at[i], g2r.at[i], g2_send.at[i], g2_recv.at[i], to_z[2])
+
+    def gnear(j):
+        return remote(gzs, gq.at[j], gz_send.at[0], gz_recv.at[0], to_z[1])
+
+    def gx(i, j):
+        return remote(gq.at[j], gq.at[j], gx_send.at[i], gx_recv.at[i], to_x)
+
+    def grad_y():
+        for k in (3, 2, 1, 0):
+            gys[k] = product(k, 1 - y).astype(bf16)
+            gy(k).start()
+
+    def grad_far():
+        for i, k in enumerate((3, 2)):
+            value = product(k, y)
+            gy(k).wait_recv()
+            g2s[i] = (value + gyr[k].astype(f32)).astype(bf16)
+            gfar(i).start()
+
+    def grad_near():
+        value = product(1, y)
+        gy(1).wait_recv()
+        gfar(0).wait_recv()
+        gzs[...] = (value + gyr[1].astype(f32) + g2r[0].astype(f32)).astype(bf16)
+        gnear(me).start()
+        value = product(0, y)
+        gy(0).wait_recv()
+        gfar(1).wait_recv()
+        gq[me] = (value + gyr[0].astype(f32) + g2r[1].astype(f32)).astype(bf16)
+        gx(0, me).start()
+
+    def grad_x():
+        gnear(jz).wait_recv()
+        gx(1, jz).start()
+
+    def tell(owner):
+        return lambda k: remote(nb.at[owner], nb.at[owner], n_send.at[k - 1], n_recv.at[k - 1], {"fs": lax.rem(f + k, F)})
+
+    def grad_out():
+        gx(0, jx).wait_recv()
+        gx(1, jd).wait_recv()
+        for q in range(4):
+            g = gq[q].astype(f32)
+            grad[q * H : (q + 1) * H, :] = g
+            square = g * g
+            folded = square[:, 0:128]
+            for lane in range(128, S, 128):
+                folded = folded + square[:, lane : lane + 128]
+            nb[f, :, q * H : (q + 1) * H] = jnp.sum(folded.T, axis=0, keepdims=True)
+        for k in range(1, F):
+            tell(f)(k).start()
+
+    both, last = (0, 1), (2,)
+    first, final = 2 - inn, 1 + inn
+
+    def send(b, pieces, k, who):
+        @pl.when(who)
+        def _():
+            for p in pieces:
+                w_first(b, p, k).start()
+
+    a_copy(0, 1).start()
+    for p in (0, 1, 2):
+        w_cross(1, p, 0).start()
+    send(1, both, 1, outer)
+    send(1, both, 2, inner)
+    a_copy(0, 0).start()
+    send(1, last, 1, outer)
+    send(1, last, 2, inner)
+    a_copy(1, 0).start()
+    send(1, (0, 1, 2), 3, inner)
+    send(1, (0, 1, 2), 2, outer)
+    send(1, (0, 1, 2), 1, inner)
+
+    serve(1, both, first, True)
+    a_zn(0)
+    a_copy(1, 1).start()
+    serve(1, last, first, True)
+    a_x(0)
+    for c in loads.values():
+        c.wait()
+    serve(1, both, 3)
+    a_d(0)
+    a_s(0)
+    normalise(0, 0, 2)
+    serve(1, last, 3)
+    normalise(0, 2, 4)
+    forward(1, fs_of(0, y), True)
+    crossed(1, both, 0)
+    forward(1, fs_of(0, 1 - y))
+    a_zn(1)
+    send(0, (0, 1, 2), 3, inner)
+    send(0, both, 1, outer)
+    a_copy(2, 0).start()
+    send(0, last, 1, outer)
+    send(0, (0, 1, 2), 2, outer)
+    send(0, (0, 1, 2), 2, inner)
+    a_x(1)
+    forward(1, fs_of(first, y))
+    crossed(1, both, first)
+    forward(1, fs_of(first, 1 - y))
+    serve(1, both, final)
+    forward(1, fs_of(3, y))
+    crossed(1, both, 3)
+    forward(1, fs_of(3, 1 - y))
+    serve(1, last, final)
+    a_copy(2, 1).start()
+    for p in (0, 1, 2):
+        w_cross(0, p, 0).start()
+    a_d(1)
+    forward(1, fs_of(final, y))
+    a_s(1)
+    for k in (0, first, 3):
+        backed(1, 1, fs_of(k, y), isinstance(k, int) and k == 0)
+        crossed(1, last, k)
+        backed(1, 1, fs_of(k, 1 - y))
+    backed(1, 1, fs_of(final, y))
+    crossed(1, both, final)
+    forward(1, fs_of(final, 1 - y))
+    crossed(1, last, final)
+    backed(1, 1, fs_of(final, 1 - y))
+    elementwise()
+    partials(1)
+    x_step(1)
+    serve(0, both, first, True)
+    z_step(1, 0)
+    z_step(1, 1)
+    send(0, both, 1, inner)
+    a_zn(2)
+    serve(0, last, first, True)
+    serve(0, both, 3)
+    a_x(2)
+
+    def to_mg(rows, wide, value):
+        acts[3, wide, mine] = value
+
+    finish(1, 0, 1, ((2, 0), (3, 1)), to_mg)
+    for kind in (0, 1, 6):
+        a_copy(3, kind).start()
+    send(0, last, 1, inner)
+    serve(0, last, 3)
+    a_d(2)
+    a_s(2)
+    normalise(2, 0, 2)
+    serve(0, both, final)
+    a_zn(3)
+    normalise(2, 2, 4)
+    a_x(3)
+    for k in (0, first, 3):
+        forward(0, fs_of(k, y), isinstance(k, int) and k == 0)
+        crossed(0, both, k)
+        forward(0, fs_of(k, 1 - y))
+    serve(0, last, final)
+    forward(0, fs_of(final, y))
+    crossed(0, both, final)
+    forward(0, fs_of(final, 1 - y))
+    hidden()
+    a_d(3)
+    a_s(3)
+    grad_y()
+    for k in (0, first, 3):
+        backed(0, 3, fs_of(k, y), isinstance(k, int) and k == 0)
+        crossed(0, last, k)
+        backed(0, 3, fs_of(k, 1 - y))
+    backed(0, 3, fs_of(final, y))
+    for i, side in enumerate((1 - r, r)):
+        sibling(1, i, side).wait_send()
+    for piece in range(4):
+        x_copy(1, piece).wait_send()
+    for piece in range(2):
+        z_copy(1, piece).wait_send()
+    crossed(0, last, final)
+    backed(0, 3, fs_of(final, 1 - y))
+    elementwise()
+    partials(0, spread)
+    grad_far()
+    spread_end()
+    grad_near()
+
+    def to_out(rows, wide, value):
+        out[rows, mine] = value
+        obs[rows, :] = value
+
+    finish(0, 2, 3, ((1, 2), (2, 1)), to_out)
+    swap = remote(obs, obr, o_send.at[0], o_recv.at[0], to_s)
+    swap.start()
+    grad_x()
+    grad_out()
+    swap.wait()
+    out[:, other] = obr[...]
+
+    for b in (1, 0):
+        for p in range(3):
+            for k in (1, 2):
+                w_first(b, p, k).wait_send()
+            for k in range(4):
+                w_cross(b, p, k).wait_send()
+
+            @pl.when(inner)
+            def _(b=b, p=p):
+                w_first(b, p, 3).wait_send()
+                w_relay(b, p).wait_send()
+
+    for i in range(4):
+        for kind in range(7 if i == 3 else 6):
+            a_copy(i, kind).wait_send()
+    for i, side in enumerate((1 - r, r)):
+        sibling(0, i, side).wait_send()
+    for piece in range(3):
+        x_copy(0, piece).wait_send()
+        z_copy(0, piece).wait_send()
+    for k in range(4):
+        gy(k).wait_send()
+    for i in range(2):
+        gfar(i).wait_send()
+    gnear(me).wait_send()
+    gx(0, me).wait_send()
+    gx(1, jz).wait_send()
+    for k in range(1, F):
+        tell(lax.rem(f + F - k, F))(k).wait_recv()
+        tell(f)(k).wait_send()
+    total = nb[0]
+    for k in range(1, F):
+        total = total + nb[k]
+    norms[...] = total
+
+
+def on_square(sizes, *arrays):
+    R, F, T, n, D, H = sizes
+    S, half, m = D // F, D // 2, 4 * n
+    dma = pltpu.SemaphoreType.DMA
+    vmem = pl.BlockSpec(memory_space=pltpu.VMEM)
+    d_input, grad, norms = pl.pallas_call(
+        functools.partial(square_kernel, sizes),
+        out_shape=(
+            jax.ShapeDtypeStruct((n, D), bf16),
+            jax.ShapeDtypeStruct((4 * H, S), f32),
+            jax.ShapeDtypeStruct((1, 4 * H), f32),
+        ),
+        in_specs=[pl.BlockSpec(memory_space=pl.ANY)] * 9,
+        out_specs=(vmem, vmem, vmem),
+        scratch_shapes=[
+            pltpu.VMEM((2, D, 2 * H), bf16),
+            pltpu.VMEM((2, H, D), bf16),
+            pltpu.VMEM((4, m, D), bf16),
+            pltpu.VMEM((m, D), bf16),
+            pltpu.VMEM((m, 2 * H), f32),
+            pltpu.VMEM((m, H), f32),
+            pltpu.VMEM((m, 2 * H), bf16),
+            pltpu.VMEM((H, m), bf16),
+            pltpu.VMEM((m, D), bf16),
+            pltpu.VMEM((2, m, half), bf16),
+            pltpu.VMEM((2 * n, half), bf16),
+            pltpu.VMEM((2, 2 * n, half), bf16),
+            pltpu.VMEM((2 * n, half), bf16),
+            pltpu.VMEM((2, 2 * n, half), bf16),
+            pltpu.VMEM((n, half), f32),
+            pltpu.VMEM((n, 128), f32),
+            pltpu.VMEM((n, 128), f32),
+            pltpu.VMEM((2, n, 128), f32),
+            pltpu.VMEM((n, half), bf16),
+            pltpu.VMEM((n, half), bf16),
+            pltpu.VMEM((4, H, S), bf16),
+            pltpu.VMEM((4, H, S), bf16),
+            pltpu.VMEM((2, H, S), bf16),
+            pltpu.VMEM((2, H, S), bf16),
+            pltpu.VMEM((H, S), bf16),
+            pltpu.VMEM((4, H, S), bf16),
+            pltpu.VMEM((F, 1, 4 * H), f32),
+            dma((9,)),
+            dma((2, 3, 4)),
+            dma((2, 3, 4)),
+            dma((2, 3, 4)),
+            dma((2, 3, 4)),
+            dma((4, 7)),
+            dma((4, 7)),
+            dma((2, 2)),
+            dma((2, 2)),
+            dma((2, 4)),
+            dma((2, 4)),
+            dma((2, 4)),
+            dma((2, 4)),
+            dma((2,)),
+            dma((2,)),
+            dma((1,)),
+            dma((1,)),
+            dma((4,)),
+            dma((4,)),
+            dma((2,)),
+            dma((2,)),
+            dma((1,)),
+            dma((1,)),
+            dma((2,)),
+            dma((2,)),
+            dma((F - 1,)),
+            dma((F - 1,)),
+        ],
+        compiler_params=pltpu.CompilerParams(
+            collective_id=0, has_side_effects=True, vmem_limit_bytes=67043328
+        ),
+    )(*arrays)
+    return d_input, grad, norms.reshape(-1)
+
+
 def solution(mesh):
     R, F, T = (mesh.shape[a] for a in ("rep", "fs", "tp"))
 
     def whole(tokens, mid_tokens, out_grad, gate_first, *rest):
         D, FF = gate_first.shape
-        sizes = (R, F, T, tokens.shape[0] // (R * F), D, FF // (T * R), 3 if F <= 8 and FF // (T * R) % 384 == 0 else 1)
+        n = tokens.shape[0] // (R * F)
+        H = FF // (T * R)
+        sizes = (R, F, T, n, D, H, 3 if F <= 8 and H % 384 == 0 else 1)
+        body = functools.partial(on_device, sizes)
+        if (R, F, T) == (2, 8, 2) and H % 256 == 0 and D % 1024 == 0 and n % 128 == 0:
+            body = functools.partial(on_square, (R, F, T, n, D, H // 2))
         return jax.shard_map(
-            functools.partial(on_device, sizes),
+            body,
             mesh=mesh,
             in_specs=(P(("rep", "fs"), None),) * 3 + (P("fs", "tp"), P("fs", "tp"), P("tp", "fs")) * 2,
             out_specs=(P(("rep", "fs"), None), P("tp", "fs"), P("tp")),

time: 244 us -> 215 us (0.88)
  Pallas kernels: 236 us -> 209 us
  local copies, waits for them, and re-layouts: 7.1 us -> 3.45 us
    pallas_call x1, Pallas kernels: 236 us -> 209 us  [on_square(): pl.pallas_call(functools.partial(square_kernel, sizes), out_shape=(jax.Sh...]
    unnamed x8 -> x4, local copies, waits for them, and re-layouts: 5.93 us -> 3.45 us
where the time goes in v1:
time: 215 us
  Pallas kernels  209 us (97%)
  local copies, waits for them, and re-layouts  3.45 us (2%)
    pallas_call x1, Pallas kernels, on_square(): pl.pallas_call(functools.partial(square_kernel, sizes), out_shape=(jax.Sh...  209 us

profile of v1, /device:TPU:0, one launch (start us, length us, event | category | flops | bytes accessed | tf_op | source)
XLA Modules:
  0.0 214.7 jit_solution(2495563367189965418)
XLA Ops:
  0.6 209.2 %shard_map.112 = (bf16[256,2048]{1,0:T(8,128)(2,1)}, f32[1536,256]{1,0:T(8,128)}, f32[1,1536]{1,0:T(1,128)}) custom-call(bf16[256,2048]{1,0:T(8,128)(2,1)} %tok.1, bf16[256,2048]{1,0:T(8,128)(2,1)} %mid.1, bf16[256,2048]{1,0:T(8,128)(2,1)} %cot.1, bf16[256,1536]{1,0:T(8,128)(2,1)} %g1.1, bf16[256,1536]{1,0:T(8,128)(2,1)} %u1_.1, bf16[1536,256]{1,0:T(8,128)(2,1)} %v1.1, ...), custom_call_target="tpu_custom_call" | custom-call | tf_op jit(solution)/shard_map/pallas_call | solution.py:936
  209.8 0.0 copy-start
  209.8 1.4 reduce
  211.3 2.3 %copy.14 = bf16[256,2048]{1,0:T(8,128)(2,1)} copy(bf16[256,2048]{1,0:T(8,128)(2,1)} %get-tuple-element.12) | data formatting | bytes 2097152
  213.6 0.0 copy-done
  213.6 1.1 copy.15
Async XLA Ops:
  209.8 3.7 %copy-start = (f32[1536,256]{1,0:T(8,128)S(1)}, f32[1536,256]{1,0:T(8,128)}, u32[]{:S(2)}) copy-start(f32[1536,256]{1,0:T(8,128)} %get-tuple-element.13) | copy-start | bytes 4718596

commit v2 on v1

--- a/solution.py
+++ b/solution.py
@@ -557,14 +557,23 @@
             value = jnp.dot(xb[:, cut], gu[b, at(owner * S, S), cols], preferred_element_type=f32)
             acc[:, cols] = value if first else acc[:, cols] + value
 
-    def backed(b, i, owner, first=False):
+    def backed(b, i, owner, blocks, fresh=False):
         cut = at(owner * S, S, 128)
 
-        @pl.loop(0, 2)
-        def _(j):
-            rows = at(j * 2 * n, 2 * n)
+        def update(rows):
             value = lax.dot_general(acts[i, rows, cut], dd[b, :, cut], nt, preferred_element_type=f32)
-            bk[rows, :] = value if first else bk[rows, :] + value
+            bk[rows, :] = value if fresh else bk[rows, :] + value
+
+        if blocks == 4:
+            @pl.loop(0, 2)
+            def _(c):
+                update(at(c * 2 * n, 2 * n))
+        elif blocks == 3:
+            @pl.loop(1, 4)
+            def _(c):
+                update(rows_of(lax.rem(jd + c, 4)))
+        else:
+            update(rows_of(jd))
 
     def hidden():
         @pl.loop(0, 4 * n // 128)
@@ -573,35 +582,33 @@
             gate = acc[rows, 0:H]
             hT[:, at(c * 128, 128, 128)] = (gate * jax.nn.sigmoid(gate) * acc[rows, H : 2 * H]).astype(bf16).T
 
-    def elementwise():
-        @pl.loop(0, 4 * n // 64)
+    def elementwise(lo, hi):
+        @pl.loop(lo * n // 64, hi * n // 64)
         def _(c):
-            rows = at(c * 64, 64)
+            block = lax.rem(jd + c // (n // 64), 4)
+            rows = at(block * n + lax.rem(c, n // 64) * 64, 64)
             gate, upper, back = acc[rows, 0:H], acc[rows, H : 2 * H], 0.5 * bk[rows, :]
             logistic = jax.nn.sigmoid(gate)
             dg[rows, 0:H] = (back * upper * logistic * (1.0 + gate * (1.0 - logistic))).astype(bf16)
             dg[rows, H : 2 * H] = (back * gate * logistic).astype(bf16)
 
-    def partial(b, side, c):
-        rows = at(side * 2 * n, 2 * n)
-
+    def partial(b, rows, c):
         @pl.loop(0, half // 256)
         def _(j):
             wide = c * half + j * 256
             total = lax.dot_general(dg[rows, :], gu[b, at(wide, 256), :], nt, preferred_element_type=f32)
             part[rows, at(wide, 256, 128)] = total.astype(bf16)
 
-    def sibling(b, i, side):
-        rows = at(side * 2 * n, 2 * n)
-        return remote(part.at[rows, other], sib.at[b, rows], s_send.at[b, i], s_recv.at[b, i], to_s)
-
-    def partials(b, between=None):
-        for i, side in enumerate((1 - r, r)):
-            partial(b, side, 1 - t)
-            sibling(b, i, side).start()
-            partial(b, side, t)
-            if between is not None:
-                between(i)
+    def group(i):
+        return (rows_of(jd), rows_of(jx), at(r * 2 * n, 2 * n))[i]
+
+    def sibling(b, i):
+        return remote(part.at[group(i), other], sib.at[b, group(i)], s_send.at[b, i], s_recv.at[b, i], to_s)
+
+    def partials(b, i):
+        partial(b, group(i), 1 - t)
+        sibling(b, i).start()
+        partial(b, group(i), t)
 
     def x_copy(b, piece):
         rows = pl.ds(piece * h, h)
@@ -614,17 +621,10 @@
     def own_sum(b, rows):
         return part[rows, mine].astype(f32) + sib[b, rows, :].astype(f32)
 
-    def x_step(b):
-        sibling(b, 0, 1 - r).wait_recv()
-        for piece in range(4):
+    def x_step(b, lo, hi):
+        for piece in range(lo, hi):
             base = (jd if piece < 2 else jx) * n + (piece % 2) * h
-
-            @pl.loop(0, h // 32)
-            def _(c, base=base, piece=piece):
-                xs[at(piece * h + c * 32, 32), :] = own_sum(b, at(base + c * 32, 32)).astype(bf16)
-
-            x_copy(b, piece).start()
-        sibling(b, 1, r).wait_recv()
+            sum_send(b, xs, piece, base, None, x_copy)
 
     def z_step(b, piece):
         x_copy(b, piece).wait_recv()
@@ -647,23 +647,16 @@
 
         copy(b, piece).start()
 
-    def spread(i):
-        sibling(0, i, (1 - r, r)[i]).wait_recv()
-        if i == 0:
-            sum_send(0, xs, 0, jd * n, None, x_copy)
-            sum_send(0, zs, 0, jd * n + h, None, z_copy)
-            sum_send(0, xs, 1, jx * n, None, x_copy)
-        else:
-            sum_send(0, zs, 1, jz * n + h, None, z_copy)
-
-    def spread_end():
+    def spread_x():
+        z_copy(0, 0).wait_recv()
+        sum_send(0, xs, 2, jx * n + h, zr, x_copy)
+
+    def spread_z():
         x_copy(0, 0).wait_recv()
         sum_send(0, zs, 2, jz * n, xr, z_copy)
-        z_copy(0, 0).wait_recv()
-        sum_send(0, xs, 2, jx * n + h, zr, x_copy)
-
-    def finish(b, ui, ci, parts, store):
-        for piece, (px, pz) in enumerate(parts):
+
+    def finish(b, ui, ci, parts, store, done):
+        for piece, px, pz in parts:
             x_copy(b, px).wait_recv()
             z_copy(b, pz).wait_recv()
 
@@ -679,18 +672,21 @@
                 ps[rows, :] = jnp.broadcast_to(jnp.sum(d * normed, axis=1, keepdims=True), (32, 128))
                 scb[rows, :] = jnp.broadcast_to(scale, (32, 128))
 
-        tell = remote(ps, pr.at[b], p_send.at[b], p_recv.at[b], to_s)
-        tell.start()
-        tell.wait()
-
-        @pl.loop(0, n // 32)
-        def _(c):
-            rows, wide = at(c * 32, 32), at(me * n + c * 32, 32)
-            scale = scb[rows, 0:1]
-            normed = acts[ui, wide, mine].astype(f32) * scale
-            mean = (ps[rows, 0:1] + pr[b, rows, 0:1]) * (1.0 / D)
-            d_u = acts[ci, wide, mine].astype(f32) + scale * (dbuf[rows, :] - normed * mean)
-            store(rows, wide, d_u.astype(bf16))
+            part_rows = pl.ds(piece * h, h)
+            tell_half = remote(ps.at[part_rows], pr.at[b, part_rows], p_send.at[b, piece], p_recv.at[b, piece], to_s)
+            tell_half.start()
+            tell_half.wait()
+
+            @pl.loop(piece * h // 32, (piece + 1) * h // 32)
+            def _(c):
+                rows, wide = at(c * 32, 32), at(me * n + c * 32, 32)
+                scale = scb[rows, 0:1]
+                normed = acts[ui, wide, mine].astype(f32) * scale
+                mean = (ps[rows, 0:1] + pr[b, rows, 0:1]) * (1.0 / D)
+                d_u = acts[ci, wide, mine].astype(f32) + scale * (dbuf[rows, :] - normed * mean)
+                store(rows, wide, d_u.astype(bf16))
+
+            done(piece)
 
     def product(k, side):
         cut = at(fs_of(k, side) * S, S, 128)
@@ -708,17 +704,15 @@
     def gx(i, j):
         return remote(gq.at[j], gq.at[j], gx_send.at[i], gx_recv.at[i], to_x)
 
-    def grad_y():
-        for k in (3, 2, 1, 0):
-            gys[k] = product(k, 1 - y).astype(bf16)
-            gy(k).start()
-
-    def grad_far():
-        for i, k in enumerate((3, 2)):
-            value = product(k, y)
-            gy(k).wait_recv()
-            g2s[i] = (value + gyr[k].astype(f32)).astype(bf16)
-            gfar(i).start()
+    def grad_y(k):
+        gys[k] = product(k, 1 - y).astype(bf16)
+        gy(k).start()
+
+    def grad_far(i, k):
+        value = product(k, y)
+        gy(k).wait_recv()
+        g2s[i] = (value + gyr[k].astype(f32)).astype(bf16)
+        gfar(i).start()
 
     def grad_near():
         value = product(1, y)
@@ -726,6 +720,8 @@
         gfar(0).wait_recv()
         gzs[...] = (value + gyr[1].astype(f32) + g2r[0].astype(f32)).astype(bf16)
         gnear(me).start()
+
+    def grad_own():
         value = product(0, y)
         gy(0).wait_recv()
         gfar(1).wait_recv()
@@ -744,16 +740,18 @@
         gx(1, jd).wait_recv()
         for q in range(4):
             g = gq[q].astype(f32)
-            grad[q * H : (q + 1) * H, :] = g
+            grad[q * H : (q + 1) * H, :] = gq[q]
             square = g * g
             folded = square[:, 0:128]
             for lane in range(128, S, 128):
                 folded = folded + square[:, lane : lane + 128]
-            nb[f, :, q * H : (q + 1) * H] = jnp.sum(folded.T, axis=0, keepdims=True)
+            row = jnp.sum(folded.T, axis=0, keepdims=True)
+            for c in range(H // 128):
+                nb[f, q * H // 128 + c, :] = row[0, c * 128 : (c + 1) * 128]
         for k in range(1, F):
             tell(f)(k).start()
 
-    both, last = (0, 1), (2,)
+    both, last, every = (0, 1), (2,), (0, 1, 2)
     first, final = 2 - inn, 1 + inn
 
     def send(b, pieces, k, who):
@@ -763,133 +761,192 @@
                 w_first(b, p, k).start()
 
     a_copy(0, 1).start()
-    for p in (0, 1, 2):
+    for p in every:
         w_cross(1, p, 0).start()
+    send(1, every, 3, inner)
+    send(1, every, 2, inner)
     send(1, both, 1, outer)
-    send(1, both, 2, inner)
     a_copy(0, 0).start()
     send(1, last, 1, outer)
-    send(1, last, 2, inner)
     a_copy(1, 0).start()
-    send(1, (0, 1, 2), 3, inner)
-    send(1, (0, 1, 2), 2, outer)
-    send(1, (0, 1, 2), 1, inner)
-
-    serve(1, both, first, True)
+    send(1, every, 1, inner)
+    send(1, every, 2, outer)
+
     a_zn(0)
     a_copy(1, 1).start()
-    serve(1, last, first, True)
+    serve(1, both, first, True)
     a_x(0)
+    a_d(0)
     for c in loads.values():
         c.wait()
-    serve(1, both, 3)
-    a_d(0)
     a_s(0)
-    normalise(0, 0, 2)
-    serve(1, last, 3)
-    normalise(0, 2, 4)
+    normalise(0, 0, 4)
     forward(1, fs_of(0, y), True)
-    crossed(1, both, 0)
-    forward(1, fs_of(0, 1 - y))
-    a_zn(1)
-    send(0, (0, 1, 2), 3, inner)
+    serve(1, last, first, True)
+    send(0, every, 3, inner)
+    send(0, both, 2, inner)
     send(0, both, 1, outer)
     a_copy(2, 0).start()
     send(0, last, 1, outer)
-    send(0, (0, 1, 2), 2, outer)
-    send(0, (0, 1, 2), 2, inner)
+    send(0, every, 2, outer)
+    serve(1, (0,), 3)
+    a_zn(1)
+    a_copy(2, 1).start()
+    serve(1, (1,), 3)
+    crossed(1, both, 0)
+    forward(1, fs_of(0, 1 - y))
     a_x(1)
     forward(1, fs_of(first, y))
     crossed(1, both, first)
     forward(1, fs_of(first, 1 - y))
     serve(1, both, final)
     forward(1, fs_of(3, y))
+    serve(1, last, 3)
+    serve(1, last, final)
+    for p in every:
+        w_cross(0, p, 0).start()
+    a_d(1)
     crossed(1, both, 3)
     forward(1, fs_of(3, 1 - y))
-    serve(1, last, final)
-    a_copy(2, 1).start()
-    for p in (0, 1, 2):
-        w_cross(0, p, 0).start()
-    a_d(1)
     forward(1, fs_of(final, y))
     a_s(1)
-    for k in (0, first, 3):
-        backed(1, 1, fs_of(k, y), isinstance(k, int) and k == 0)
-        crossed(1, last, k)
-        backed(1, 1, fs_of(k, 1 - y))
-    backed(1, 1, fs_of(final, y))
+    backed(1, 1, fs_of(0, y), 4, True)
+    crossed(1, last, 0)
+    backed(1, 1, fs_of(0, 1 - y), 4)
+    backed(1, 1, fs_of(first, y), 4)
+    crossed(1, last, first)
+    backed(1, 1, fs_of(first, 1 - y), 4)
+    backed(1, 1, fs_of(3, y), 4)
+    backed(1, 1, fs_of(final, y), 4)
     crossed(1, both, final)
     forward(1, fs_of(final, 1 - y))
+    crossed(1, last, 3)
+    backed(1, 1, fs_of(3, 1 - y), 4)
     crossed(1, last, final)
-    backed(1, 1, fs_of(final, 1 - y))
-    elementwise()
-    partials(1)
-    x_step(1)
-    serve(0, both, first, True)
+    backed(1, 1, fs_of(final, 1 - y), 4)
+    elementwise(0, 1)
+    partials(1, 0)
+    elementwise(1, 4)
+    sibling(1, 0).wait_recv()
+    x_step(1, 0, 2)
+    partials(1, 1)
+    sibling(1, 1).wait_recv()
+    x_step(1, 2, 4)
+    partials(1, 2)
+    sibling(1, 2).wait_recv()
     z_step(1, 0)
+    a_zn(2)
     z_step(1, 1)
-    send(0, both, 1, inner)
-    a_zn(2)
-    serve(0, last, first, True)
-    serve(0, both, 3)
+    send(0, last, 2, inner)
+    serve(0, every, first, True)
     a_x(2)
 
     def to_mg(rows, wide, value):
         acts[3, wide, mine] = value
 
-    finish(1, 0, 1, ((2, 0), (3, 1)), to_mg)
-    for kind in (0, 1, 6):
+    finish(1, 0, 1, ((0, 2, 0), (1, 3, 1)), to_mg, lambda piece: None)
+    for kind in (1, 0, 6):
         a_copy(3, kind).start()
-    send(0, last, 1, inner)
-    serve(0, last, 3)
+    send(0, every, 1, inner)
+    serve(0, every, 3)
+
+    @pl.when(inner)
+    def _():
+        serve(0, every, 2)
+
     a_d(2)
     a_s(2)
-    normalise(2, 0, 2)
-    serve(0, both, final)
+    normalise(2, 0, 4)
     a_zn(3)
-    normalise(2, 2, 4)
-    a_x(3)
-    for k in (0, first, 3):
-        forward(0, fs_of(k, y), isinstance(k, int) and k == 0)
+    for k in (0, first):
+        forward(0, fs_of(k, y), isinstance(k, int))
         crossed(0, both, k)
         forward(0, fs_of(k, 1 - y))
-    serve(0, last, final)
+    @pl.when(outer)
+    def _():
+        serve(0, (0,), 1)
+
+    a_x(3)
+    forward(0, fs_of(3, y))
+    crossed(0, both, 3)
+    forward(0, fs_of(3, 1 - y))
+    @pl.when(outer)
+    def _():
+        serve(0, (1,), 1)
+
+    for kind in (6, 3, 4):
+        a_arrived(3, kind)
+    for k in (0, first):
+        backed(0, 3, fs_of(k, y), 3, isinstance(k, int))
+        crossed(0, last, k)
+        backed(0, 3, fs_of(k, 1 - y), 3)
+    @pl.when(outer)
+    def _():
+        serve(0, last, 1)
+
+    backed(0, 3, fs_of(3, y), 3)
+    crossed(0, last, 3)
+    backed(0, 3, fs_of(3, 1 - y), 3)
     forward(0, fs_of(final, y))
     crossed(0, both, final)
     forward(0, fs_of(final, 1 - y))
     hidden()
     a_d(3)
-    a_s(3)
-    grad_y()
-    for k in (0, first, 3):
-        backed(0, 3, fs_of(k, y), isinstance(k, int) and k == 0)
-        crossed(0, last, k)
-        backed(0, 3, fs_of(k, 1 - y))
-    backed(0, 3, fs_of(final, y))
-    for i, side in enumerate((1 - r, r)):
-        sibling(1, i, side).wait_send()
+    for i in range(3):
+        sibling(1, i).wait_send()
     for piece in range(4):
         x_copy(1, piece).wait_send()
     for piece in range(2):
         z_copy(1, piece).wait_send()
+    a_arrived(3, 5)
+    grad_y(3)
+    for k in (0, first, 3):
+        for side in (y, 1 - y):
+            backed(0, 3, fs_of(k, side), 1, isinstance(k, int) and k == 0 and side is y)
+    backed(0, 3, fs_of(final, y), 1)
     crossed(0, last, final)
-    backed(0, 3, fs_of(final, 1 - y))
-    elementwise()
-    partials(0, spread)
-    grad_far()
-    spread_end()
+    backed(0, 3, fs_of(final, 1 - y), 1)
+    elementwise(0, 1)
+    partials(0, 0)
+    grad_y(2)
+    sibling(0, 0).wait_recv()
+    sum_send(0, xs, 0, jd * n, None, x_copy)
+    sum_send(0, zs, 0, jd * n + h, None, z_copy)
+    grad_far(0, 3)
+    grad_y(1)
+    backed(0, 3, fs_of(final, y), 3)
+    backed(0, 3, fs_of(final, 1 - y), 3)
+    elementwise(1, 4)
+    partials(0, 1)
+    grad_far(1, 2)
+    sibling(0, 1).wait_recv()
+    sum_send(0, xs, 1, jx * n, None, x_copy)
+    grad_y(0)
+    partials(0, 2)
+    spread_x()
     grad_near()
+    sibling(0, 2).wait_recv()
+    sum_send(0, zs, 1, jz * n + h, None, z_copy)
+    spread_z()
+    grad_own()
+    grad_x()
 
     def to_out(rows, wide, value):
         out[rows, mine] = value
         obs[rows, :] = value
 
-    finish(0, 2, 3, ((1, 2), (2, 1)), to_out)
-    swap = remote(obs, obr, o_send.at[0], o_recv.at[0], to_s)
-    swap.start()
-    grad_x()
-    grad_out()
-    swap.wait()
+    def swap(piece):
+        rows = pl.ds(piece * h, h)
+        return remote(obs.at[rows], obr.at[rows], o_send.at[piece], o_recv.at[piece], to_s)
+
+    def half_done(piece):
+        swap(piece).start()
+        if piece == 1:
+            grad_out()
+
+    finish(0, 2, 3, ((1, 2, 1), (0, 1, 2)), to_out, half_done)
+    for piece in (1, 0):
+        swap(piece).wait()
     out[:, other] = obr[...]
 
     for b in (1, 0):
@@ -907,8 +964,8 @@
     for i in range(4):
         for kind in range(7 if i == 3 else 6):
             a_copy(i, kind).wait_send()
-    for i, side in enumerate((1 - r, r)):
-        sibling(0, i, side).wait_send()
+    for i in range(3):
+        sibling(0, i).wait_send()
     for piece in range(3):
         x_copy(0, piece).wait_send()
         z_copy(0, piece).wait_send()
@@ -937,8 +994,8 @@
         functools.partial(square_kernel, sizes),
         out_shape=(
             jax.ShapeDtypeStruct((n, D), bf16),
-            jax.ShapeDtypeStruct((4 * H, S), f32),
-            jax.ShapeDtypeStruct((1, 4 * H), f32),
+            jax.ShapeDtypeStruct((4 * H, S), bf16),
+            jax.ShapeDtypeStruct((4 * H // 128, 128), f32),
         ),
         in_specs=[pl.BlockSpec(memory_space=pl.ANY)] * 9,
         out_specs=(vmem, vmem, vmem),
@@ -969,7 +1026,7 @@
             pltpu.VMEM((2, H, S), bf16),
             pltpu.VMEM((H, S), bf16),
             pltpu.VMEM((4, H, S), bf16),
-            pltpu.VMEM((F, 1, 4 * H), f32),
+            pltpu.VMEM((F, 4 * H // 128, 128), f32),
             dma((9,)),
             dma((2, 3, 4)),
             dma((2, 3, 4)),
@@ -977,16 +1034,16 @@
             dma((2, 3, 4)),
             dma((4, 7)),
             dma((4, 7)),
-            dma((2, 2)),
-            dma((2, 2)),
+            dma((2, 3)),
+            dma((2, 3)),
             dma((2, 4)),
             dma((2, 4)),
             dma((2, 4)),
             dma((2, 4)),
+            dma((2, 2)),
+            dma((2, 2)),
             dma((2,)),
             dma((2,)),
-            dma((1,)),
-            dma((1,)),
             dma((4,)),
             dma((4,)),
             dma((2,)),
@@ -1002,7 +1059,7 @@
             collective_id=0, has_side_effects=True, vmem_limit_bytes=67043328
         ),
     )(*arrays)
-    return d_input, grad, norms.reshape(-1)
+    return d_input, grad.astype(f32), norms.reshape(-1)
 
 
 def solution(mesh):

time: 215 us -> 205 us (0.953)
  Pallas kernels: 209 us -> 200 us
    pallas_call x1, Pallas kernels: 209 us -> 200 us  [on_square(): pl.pallas_call(functools.partial(square_kernel, sizes), out_shape=(jax.Sh...]
    convert_element_type x0 -> x1, other arithmetic: none -> 2.48 us  [on_square(): return (d_input, grad.astype(f32), norms.reshape(-1))]
where the time goes in v2:
time: 205 us
  Pallas kernels  200 us (98%)
  other arithmetic  2.48 us (1%)
    pallas_call x1, Pallas kernels, on_square(): pl.pallas_call(functools.partial(square_kernel, sizes), out_shape=(jax.Sh...  200 us

profile of v2, /device:TPU:0, one launch (start us, length us, event | category | flops | bytes accessed | tf_op | source)
XLA Modules:
  0.0 205.1 jit_solution(13428114199893052128)
XLA Ops:
  0.6 200.4 %shard_map.112 = (bf16[256,2048]{1,0:T(8,128)(2,1)}, bf16[1536,256]{1,0:T(8,128)(2,1)}, f32[12,128]{1,0:T(8,128)}) custom-call(bf16[256,2048]{1,0:T(8,128)(2,1)} %tok.1, bf16[256,2048]{1,0:T(8,128)(2,1)} %mid.1, bf16[256,2048]{1,0:T(8,128)(2,1)} %cot.1, bf16[256,1536]{1,0:T(8,128)(2,1)} %g1.1, bf16[256,1536]{1,0:T(8,128)(2,1)} %u1_.1, bf16[1536,256]{1,0:T(8,128)(2,1)} %v1.1, ...), custom_call_target="tpu_custom_call" | custom-call | tf_op jit(solution)/shard_map/pallas_call | solution.py:993
  201.1 0.0 copy-start
  201.1 2.5 %convert_element_type.3 = f32[1536,256]{1,0:T(8,128)} convert(bf16[1536,256]{1,0:T(8,128)(2,1)} %get-tuple-element.7) | non-fusion elementwise | flops 393216 | bytes 2359296 | tf_op jit(solution)/shard_map/convert_element_type | solution.py:1062
  203.6 0.0 copy-done
  203.6 0.0 copy-start.1
  203.6 1.0 copy.14
  204.5 0.0 copy-done.1
  204.5 0.6 copy.15
Async XLA Ops:
  201.1 2.5 %copy-start = (bf16[256,2048]{1,0:T(8,128)(2,1)S(1)}, bf16[256,2048]{1,0:T(8,128)(2,1)}, u32[]{:S(2)}) copy-start(bf16[256,2048]{1,0:T(8,128)(2,1)} %get-tuple-element.12) | copy-start | bytes 3145732
  203.6 1.0 copy-start.1
